TPU v7x, 32 devices: a whole 2x2x4 slice. The times are simulated.
32 devices in a mesh: tp: 16 (over z, y, x), dp: 2 (over core).
Axes of the slice: x: 2, y: 2, z: 4, core: 2. Of those that a mesh axis runs over, the one named last changes fastest.
Arguments:
- tokens: bfloat16 [256, 4096], P(None, 'dp'), may hold values from -20 to 20
- norm_gain: float32 [2, 4096], P(None, 'dp'), may hold values from 0.1 to 1.9
- receptance: bfloat16 [2, 4096, 1024], P(None, 'dp', 'tp'), may hold values from -0.09375 to 0.09375
- key_proj: bfloat16 [2, 4096, 1024], P(None, 'dp', 'tp'), may hold values from -0.09375 to 0.09375
- value_proj: bfloat16 [2, 4096, 1024], P(None, 'dp', 'tp'), may hold values from -0.09375 to 0.09375
- decay_proj: bfloat16 [2, 4096, 1024], P(None, 'dp', 'tp'), may hold values from -0.09375 to 0.09375
- rate_proj: bfloat16 [2, 4096, 1024], P(None, 'dp', 'tp'), may hold values from -0.09375 to 0.09375
- gate_proj: bfloat16 [2, 4096, 1024], P(None, 'dp', 'tp'), may hold values from -0.09375 to 0.09375
- decay_base: float32 [2, 1024], P(None, 'tp'), may hold values from -6 to 1
- group_gain: float32 [2, 1024], P(None, 'tp'), may hold values from 0.1 to 1.9
- output_proj: bfloat16 [2, 1024, 4096], P(None, 'tp', 'dp'), may hold values from -0.1875 to 0.1875
- state: float32 [2, 256, 16, 4096], P(None, 'dp', 'tp'), may hold values from -3 to 3
Outputs:
- next_tokens: bfloat16 [256, 4096], P(None, 'dp')
- new_state: float32 [2, 256, 16, 4096], P(None, 'dp', 'tp')
All inputs are finite; a program needn't handle non-finite values.
Results may differ from a plain program's by a relative error of at most 0.0066.
Values may be sent and summed in bfloat16 or wider, within the bound.
No kernel may reach another device: no remote copies, remote signals or barrier semaphores. Data moves between devices by JAX's collectives and lax.ppermute only.
A program may use at most 64 MiB of HBM per device.

v0:
```python
import jax
import jax.numpy as jnp
from jax import lax
from jax.sharding import PartitionSpec as P

D = 4096
HEAD = 64
LAYERS = 2
norm_floor = 0.1
group_floor = 0.5


def recurrence(state_block, recept_heads, key_heads, value_heads, decay_heads, rate_heads):
    log_rate = -jax.nn.softplus(-decay_heads) - 0.5
    forget = jnp.exp(-jnp.exp(log_rate))
    learn_rate = jax.nn.sigmoid(rate_heads)
    unit_key = key_heads * lax.rsqrt(jnp.sum(key_heads * key_heads, axis=-1, keepdims=True) + 1.0)
    scaled = key_heads * learn_rate
    removed = jnp.einsum("bhvk,bhk->bhv", state_block, -unit_key, precision=lax.Precision.HIGHEST)
    updated = (
        state_block * forget[:, :, None, :]
        + removed[..., None] * (unit_key * learn_rate)[:, :, None, :]
        + value_heads[..., None] * scaled[:, :, None, :]
    )
    read_out = jnp.einsum("bhvk,bhk->bhv", updated, recept_heads, precision=lax.Precision.HIGHEST)
    centre = read_out - jnp.mean(read_out, axis=-1, keepdims=True)
    normal = centre * lax.rsqrt(jnp.mean(centre * centre, axis=-1, keepdims=True) + group_floor)
    return (updated, normal)


def shards(
    tokens,
    norm_gain,
    receptance,
    key_proj,
    value_proj,
    decay_proj,
    rate_proj,
    gate_proj,
    decay_base,
    group_gain,
    output_proj,
    state,
):
    local_rows = state.shape[1]
    first_row = lax.axis_index("dp") * local_rows
    local_heads = state.shape[2]
    current = tokens
    finals = []
    for section_index in range(LAYERS):
        floats = current.astype(jnp.float32)
        squares = jnp.sum(floats * floats, axis=1)
        normed = (floats * norm_gain[section_index]).astype(jnp.bfloat16)
        part_recept = jnp.dot(normed, receptance[section_index], preferred_element_type=jnp.float32)
        part_key = jnp.dot(normed, key_proj[section_index], preferred_element_type=jnp.float32)
        part_value = jnp.dot(normed, value_proj[section_index], preferred_element_type=jnp.float32)
        part_decay = jnp.dot(normed, decay_proj[section_index], preferred_element_type=jnp.float32)
        part_rate = jnp.dot(normed, rate_proj[section_index], preferred_element_type=jnp.float32)
        part_gate = jnp.dot(normed, gate_proj[section_index], preferred_element_type=jnp.float32)
        totals = lax.psum(squares, "dp")
        own_squares = lax.dynamic_slice_in_dim(totals, first_row, local_rows, 0)
        summed = (
            lax.psum_scatter(part_recept, "dp", scatter_dimension=0, tiled=True),
            lax.psum_scatter(part_key, "dp", scatter_dimension=0, tiled=True),
            lax.psum_scatter(part_value, "dp", scatter_dimension=0, tiled=True),
            lax.psum_scatter(part_decay, "dp", scatter_dimension=0, tiled=True),
            lax.psum_scatter(part_rate, "dp", scatter_dimension=0, tiled=True),
            lax.psum_scatter(part_gate, "dp", scatter_dimension=0, tiled=True),
        )
        inv_rms = lax.rsqrt(own_squares / D + norm_floor)

        def by_head(term):
            rounded = lax.optimization_barrier((inv_rms[:, None] * term).astype(jnp.bfloat16))
            return rounded.astype(jnp.float32).reshape(local_rows, local_heads, HEAD)

        decay_heads = by_head(summed[3]) + decay_base[section_index].reshape(1, local_heads, HEAD)
        updated, normal = recurrence(
            state[section_index].reshape(local_rows, local_heads, HEAD, HEAD),
            by_head(summed[0]),
            by_head(summed[1]),
            by_head(summed[2]),
            decay_heads,
            by_head(summed[4]),
        )
        finals.append(updated.reshape(local_rows, local_heads, HEAD * HEAD))
        gate_value = jax.nn.sigmoid(by_head(summed[5]).reshape(local_rows, local_heads * HEAD))
        mixed_heads = (
            normal.reshape(local_rows, local_heads * HEAD) * group_gain[section_index] * gate_value
        ).astype(jnp.bfloat16)
        weights_out = output_proj[section_index]

        def apply_out(piece, begin, weights_out=weights_out):
            return jnp.dot(piece, weights_out, preferred_element_type=jnp.float32)

        partial_out = apply_out(lax.all_gather(mixed_heads, "dp", axis=0, tiled=True), jnp.int32(0))
        total = lax.psum(partial_out, "tp")
        current = (floats + total).astype(jnp.bfloat16)
    return (current, jnp.stack(finals))


def solution(mesh):
    return jax.shard_map(
        shards,
        mesh=mesh,
        in_specs=(
            P(None, "dp"),
            P(None, "dp"),
            P(None, "dp", "tp"),
            P(None, "dp", "tp"),
            P(None, "dp", "tp"),
            P(None, "dp", "tp"),
            P(None, "dp", "tp"),
            P(None, "dp", "tp"),
            P(None, "tp"),
            P(None, "tp"),
            P(None, "tp", "dp"),
            P(None, "dp", "tp", None),
        ),
        out_specs=(P(None, "dp"), P(None, "dp", "tp", None)),
        check_vma=False,
    )
```

profile of v0, /device:TPU:0, one launch (start us, length us, event | category | flops | bytes accessed | tf_op | source)
XLA Modules:
  0.0 421.7 jit_solution(14630838087907600654)
XLA Ops:
  8.1 2.3 fusion.22
  10.5 2.4 fusion.26
  17.6 8.1 %fusion.77 = (f32[1,128,1,4096]{3,2,1,0:T(1,128)}, f32[1,128,1,4096]{3,2,1,0:T(1,128)}) fusion(f32[2,128,1,4096]{3,2,1,0:T(1,128)} %param.23), kind=kLoop, calls=%fused_computation.119 | loop fusion | bytes 8388608 | tf_op jit(solution)/shard_map/slice | solution.py:78
  26.0 5.0 %copy.45 = f32[1,128,1,4096]{1,3,2,0:T(8,128)S(1)} copy(f32[1,128,1,4096]{3,2,1,0:T(1,128)} %get-tuple-element.7) | data formatting | bytes 4194304
  31.1 2.6 psum.28
  33.8 9.1 %reduce-scatter.17.cloned.1.call-done = f32[128,64]{0,1:T(8,128)} async-done(((f32[256,64]{0,1:T(8,128)}), f32[128,64]{0,1:T(8,128)}) %reduce-scatter.17.cloned.1.call-update) | async-done | bytes 32784 | tf_op jit(solution)/shard_map/reduce_scatter | solution.py:67
  42.8 10.7 %reduce-scatter.21.cloned.1.call-done = f32[128,64]{0,1:T(8,128)} async-done(((f32[256,64]{0,1:T(8,128)}), f32[128,64]{0,1:T(8,128)}) %reduce-scatter.21.cloned.1.call-update) | async-done | bytes 32784 | tf_op jit(solution)/shard_map/reduce_scatter | solution.py:63
  53.6 10.7 %reduce-scatter.23.cloned.1.call-done = f32[128,64]{0,1:T(8,128)} async-done(((f32[256,64]{0,1:T(8,128)}), f32[128,64]{0,1:T(8,128)}) %reduce-scatter.23.cloned.1.call-update) | async-done | bytes 32784 | tf_op jit(solution)/shard_map/reduce_scatter | solution.py:68
  64.3 10.7 %reduce-scatter.13.cloned.1.call-done = f32[128,64]{0,1:T(8,128)} async-done(((f32[256,64]{0,1:T(8,128)}), f32[128,64]{0,1:T(8,128)}) %reduce-scatter.13.cloned.1.call-update) | async-done | bytes 32784 | tf_op jit(solution)/shard_map/reduce_scatter | solution.py:66
  79.2 2.7 fusion.38
  82.0 5.6 %copy.46 = f32[1,128,1,4096]{1,3,2,0:T(8,128)} copy(f32[1,128,1,4096]{3,2,1,0:T(1,128)} %get-tuple-element.6) | data formatting | bytes 4194304
  87.7 122.2 %all-reduce.3.cloned.1.call-done = f32[256,2048]{1,0:T(8,128)} async-done(((f32[256,2048]{1,0:T(8,128)}), f32[256,2048]{1,0:T(8,128)}) %all-reduce.3.cloned.1.call-update) | async-done | bytes 2097168 | tf_op jit(solution)/shard_map/psum | solution.py:96
  214.0 2.4 fusion.14
  216.5 2.3 fusion.12
  225.2 2.6 broadcast_multiply_fusion.2
  227.8 2.6 psum.30
  231.9 10.7 %reduce-scatter.29.cloned.1.call-done = f32[128,64]{0,1:T(8,128)} async-done(((f32[256,64]{0,1:T(8,128)}), f32[128,64]{0,1:T(8,128)}) %reduce-scatter.29.cloned.1.call-update) | async-done | bytes 32784 | tf_op jit(solution)/shard_map/reduce_scatter | solution.py:67
  242.6 11.5 %reduce-scatter.33.cloned.1.call-done = f32[128,64]{0,1:T(8,128)} async-done(((f32[256,64]{0,1:T(8,128)}), f32[128,64]{0,1:T(8,128)}) %reduce-scatter.33.cloned.1.call-update) | async-done | bytes 32784 | tf_op jit(solution)/shard_map/reduce_scatter | solution.py:63
  254.1 10.7 %reduce-scatter.35.cloned.1.call-done = f32[128,64]{0,1:T(8,128)} async-done(((f32[256,64]{0,1:T(8,128)}), f32[128,64]{0,1:T(8,128)}) %reduce-scatter.35.cloned.1.call-update) | async-done | bytes 32784 | tf_op jit(solution)/shard_map/reduce_scatter | solution.py:68
  264.8 10.9 %reduce-scatter.25.cloned.1.call-done = f32[128,64]{0,1:T(8,128)} async-done(((f32[256,64]{0,1:T(8,128)}), f32[128,64]{0,1:T(8,128)}) %reduce-scatter.25.cloned.1.call-update) | async-done | bytes 32784 | tf_op jit(solution)/shard_map/reduce_scatter | solution.py:66
  281.7 2.7 fusion.30
  292.9 10.1 %copy.24 = f32[2,128,1,4096]{3,2,1,0:T(1,128)} copy(f32[2,128,1,4096]{1,3,2,0:T(8,128)} %pad_maximum_fusion) | data formatting | bytes 8388608
  303.1 109.3 %all-reduce.5.cloned.1.call-done = f32[256,2048]{1,0:T(8,128)} async-done(((f32[256,2048]{1,0:T(8,128)}), f32[256,2048]{1,0:T(8,128)}) %all-reduce.5.cloned.1.call-update) | async-done | bytes 2097168 | tf_op jit(solution)/shard_map/psum | solution.py:96
  412.4 2.8 fusion.5
  (109 shorter events, 36.4 us)
Async XLA Ops:
  7.2 5.8 %copy-start.3 = (bf16[256,2048]{1,0:T(8,128)(2,1)S(1)}, bf16[256,2048]{1,0:T(8,128)(2,1)}, u32[]{:S(2)}) copy-start(bf16[256,2048]{1,0:T(8,128)(2,1)} %param.12) | copy-start | bytes 3145732
  7.2 5.8 %copy-start.9 = (bf16[2,2048,64]{1,2,0:T(8,128)(2,1)S(1)}, bf16[2,2048,64]{1,2,0:T(8,128)(2,1)}, u32[]{:S(2)}) copy-start(bf16[2,2048,64]{1,2,0:T(8,128)(2,1)} %param.18) | copy-start | bytes 1572868
  7.2 26.6 %reduce-scatter.19.cloned.1.call-start = ((), (), s32[]{:S(2)}) async-start(), calls=%async_computation.15 | async-start | bytes 98304 | tf_op jit(solution)/shard_map/reduce_scatter | solution.py:65
  10.4 3.7 copy-start.10
  10.5 23.3 %reduce-scatter.15.cloned.1.call-start = ((), (), s32[]{:S(2)}) async-start(), calls=%async_computation.13 | async-start | bytes 98304 | tf_op jit(solution)/shard_map/reduce_scatter | solution.py:64
  12.9 2.4 copy-start.11
  12.9 29.9 %reduce-scatter.17.cloned.1.call-start = ((), (), s32[]{:S(2)}) async-start(), calls=%async_computation.14 | async-start | bytes 98304 | tf_op jit(solution)/shard_map/reduce_scatter | solution.py:67
  14.1 2.4 copy-start.12
  14.1 39.5 %reduce-scatter.21.cloned.1.call-start = ((), (), s32[]{:S(2)}) async-start(), calls=%async_computation.16 | async-start | bytes 98304 | tf_op jit(solution)/shard_map/reduce_scatter | solution.py:63
  15.2 49.1 %reduce-scatter.23.cloned.1.call-start = ((), (), s32[]{:S(2)}) async-start(), calls=%async_computation.17 | async-start | bytes 98304 | tf_op jit(solution)/shard_map/reduce_scatter | solution.py:68
  16.4 58.7 %reduce-scatter.13.cloned.1.call-start = ((), (), s32[]{:S(2)}) async-start(), calls=%async_computation.12 | async-start | bytes 98304 | tf_op jit(solution)/shard_map/reduce_scatter | solution.py:66
  17.5 8.2 %copy-start.6 = (f32[2,64]{1,0:T(2,128)S(1)}, f32[2,64]{1,0:T(2,128)}, u32[]{:S(2)}) copy-start(f32[2,64]{1,0:T(2,128)} %param.20) | copy-start | bytes 1540
  17.6 8.1 %copy-start.7 = (f32[2,64]{1,0:T(2,128)S(1)}, f32[2,64]{1,0:T(2,128)}, u32[]{:S(2)}) copy-start(f32[2,64]{1,0:T(2,128)} %param.21) | copy-start | bytes 1540
  17.6 192.3 %all-reduce.3.cloned.1.call-start = ((), (), s32[]{:S(2)}) async-start(), calls=%async_computation.18 | async-start | bytes 4194304 | tf_op jit(solution)/shard_map/psum | solution.py:96
  82.0 148.6 %reduce-scatter.31.cloned.1.call-start = ((), (), s32[]{:S(2)}) async-start(), calls=%async_computation.22 | async-start | bytes 98304 | tf_op jit(solution)/shard_map/reduce_scatter | solution.py:65
  209.9 3.0 copy-start.8
  214.0 5.0 %copy-start.5 = (bf16[256,2048]{1,0:T(8,128)(2,1)S(1)}, bf16[256,2048]{1,0:T(8,128)(2,1)}, u32[]{:S(2)}) copy-start(bf16[256,2048]{1,0:T(8,128)(2,1)} %copy-done.4) | copy-start | bytes 3145732
  214.0 17.9 %reduce-scatter.27.cloned.1.call-start = ((), (), s32[]{:S(2)}) async-start(), calls=%async_computation.20 | async-start | bytes 98304 | tf_op jit(solution)/shard_map/reduce_scatter | solution.py:64
  216.5 26.1 %reduce-scatter.29.cloned.1.call-start = ((), (), s32[]{:S(2)}) async-start(), calls=%async_computation.21 | async-start | bytes 98304 | tf_op jit(solution)/shard_map/reduce_scatter | solution.py:67
  218.9 35.2 %reduce-scatter.33.cloned.1.call-start = ((), (), s32[]{:S(2)}) async-start(), calls=%async_computation.23 | async-start | bytes 98304 | tf_op jit(solution)/shard_map/reduce_scatter | solution.py:63
  221.0 43.8 %reduce-scatter.35.cloned.1.call-start = ((), (), s32[]{:S(2)}) async-start(), calls=%async_computation.24 | async-start | bytes 98304 | tf_op jit(solution)/shard_map/reduce_scatter | solution.py:68
  223.1 52.6 %reduce-scatter.25.cloned.1.call-start = ((), (), s32[]{:S(2)}) async-start(), calls=%async_computation.19 | async-start | bytes 98304 | tf_op jit(solution)/shard_map/reduce_scatter | solution.py:66
  225.2 187.2 %all-reduce.5.cloned.1.call-start = ((), (), s32[]{:S(2)}) async-start(), calls=%async_computation.25 | async-start | bytes 4194304 | tf_op jit(solution)/shard_map/psum | solution.py:96
  275.7 3.2 copy-start
  (3 other events, 4.2 us)
Sparse Core Ops, SparseCore 0:
  10.8 10.2 reduce-scatter.18
  23.2 8.6 reduce-scatter.14
  34.2 8.6 reduce-scatter.16
  44.9 8.6 reduce-scatter.20
  55.6 8.6 reduce-scatter.22
  66.4 8.6 reduce-scatter.12
  82.1 127.7 all-reduce.2
  214.1 6.7 reduce-scatter.30
  223.1 8.7 reduce-scatter.26
  233.9 8.6 reduce-scatter.28
  245.4 8.6 reduce-scatter.32
  256.1 8.6 reduce-scatter.34
  267.0 8.6 reduce-scatter.24
  284.6 127.7 all-reduce.4
where the time goes:
time: 423 us; the launch traced here: 422 us
  waiting for transfers between devices  318 us (75%)
  local copies, waits for them, and re-layouts  33.9 us (8%)
  matrix products  26.4 us (6%)
  other arithmetic  19.5 us (5%)
  between operations  14.2 us (3%)
  blocking collectives  8.96 us (2%)
    psum x2, waiting for transfers between devices, shards(): total = lax.psum(partial_out, 'tp')  231 us
    unnamed x29, local copies, waits for them, and re-layouts  24.5 us
    reduce_scatter x2, waiting for transfers between devices, shards(): lax.psum_scatter(part_recept, 'dp', scatter_dimension=0, tiled=True)  22.2 us
    reduce_scatter x2, waiting for transfers between devices, shards(): lax.psum_scatter(part_decay, 'dp', scatter_dimension=0, tiled=True)  21.6 us
    reduce_scatter x2, waiting for transfers between devices, shards(): lax.psum_scatter(part_gate, 'dp', scatter_dimension=0, tiled=True)  21.5 us
    reduce_scatter x2, waiting for transfers between devices, shards(): lax.psum_scatter(part_rate, 'dp', scatter_dimension=0, tiled=True)  19.8 us
  transfers between devices with their start and end apart: 14, of which 11 were waited for; matrix products, arithmetic and copies ran while one was open for 13% of the time, Pallas kernels for 0%

commit v1 on v0

--- a/solution.py
+++ b/solution.py
@@ -93,7 +93,9 @@
             return jnp.dot(piece, weights_out, preferred_element_type=jnp.float32)
 
         partial_out = apply_out(lax.all_gather(mixed_heads, "dp", axis=0, tiled=True), jnp.int32(0))
-        total = lax.psum(partial_out, "tp")
+        total = partial_out
+        for hop in (1, 2, 4, 8):
+            total = total + lax.ppermute(total, "tp", [(dev, dev ^ hop) for dev in range(16)])
         current = (floats + total).astype(jnp.bfloat16)
     return (current, jnp.stack(finals))
 

time: 423 us -> 634 us (1.50)
  waiting for transfers between devices: 318 us -> 519 us
  starting transfers between devices: 0.58 us -> 16.7 us
    ppermute x0 -> x8, waiting for transfers between devices: none -> 433 us  [shards(): lax.ppermute(total, 'tp', [(dev, dev ^ hop) for dev in range(16)])]
    psum x2 -> x0, waiting for transfers between devices: 231 us -> none  [shards(): total = lax.psum(partial_out, 'tp')]
    ppermute x0 -> x8, starting transfers between devices: none -> 16.1 us  [shards(): lax.ppermute(total, 'tp', [(dev, dev ^ hop) for dev in range(16)])]
    unnamed x29 -> x27, local copies, waits for them, and re-layouts: 24.5 us -> 23.2 us
  transfers between devices with their start and end apart: 14 -> 20, of which waited for: 11 -> 17; matrix products, arithmetic and copies ran while one was open for 13% -> 8% of each run, Pallas kernels for 0% -> 0%
where the time goes in v1:
time: 634 us; the launch traced here: 633 us
  waiting for transfers between devices  519 us (82%)
  local copies, waits for them, and re-layouts  32.6 us (5%)
  matrix products  23.7 us (4%)
  other arithmetic  18.4 us (3%)
  starting transfers between devices  16.7 us (3%)
  between operations  14.5 us (2%)
  blocking collectives  8.78 us (1%)
    ppermute x8, waiting for transfers between devices, shards(): lax.ppermute(total, 'tp', [(dev, dev ^ hop) for dev in range(16)])  433 us
    unnamed x27, local copies, waits for them, and re-layouts  23.2 us
    reduce_scatter x2, waiting for transfers between devices, shards(): lax.psum_scatter(part_recept, 'dp', scatter_dimension=0, tiled=True)  22 us
    reduce_scatter x2, waiting for transfers between devices, shards(): lax.psum_scatter(part_gate, 'dp', scatter_dimension=0, tiled=True)  21.6 us
    reduce_scatter x2, waiting for transfers between devices, shards(): lax.psum_scatter(part_decay, 'dp', scatter_dimension=0, tiled=True)  21.5 us
    reduce_scatter x2, waiting for transfers between devices, shards(): lax.psum_scatter(part_rate, 'dp', scatter_dimension=0, tiled=True)  20 us
    ppermute x8, starting transfers between devices, shards(): lax.ppermute(total, 'tp', [(dev, dev ^ hop) for dev in range(16)])  16.1 us
  transfers between devices with their start and end apart: 20, of which 17 were waited for; matrix products, arithmetic and copies ran while one was open for 8% of the time, Pallas kernels for 0%

profile of v1, /device:TPU:0, one launch (start us, length us, event | category | flops | bytes accessed | tf_op | source)
XLA Modules:
  0.0 633.3 jit_solution(6865565624077744271)
XLA Ops:
  17.6 8.1 %fusion.77 = (f32[1,128,1,4096]{3,2,1,0:T(1,128)}, f32[1,128,1,4096]{3,2,1,0:T(1,128)}) fusion(f32[2,128,1,4096]{3,2,1,0:T(1,128)} %param.23), kind=kLoop, calls=%fused_computation.119 | loop fusion | bytes 8388608 | tf_op jit(solution)/shard_map/slice | solution.py:78
  26.0 5.0 copy.45
  31.1 2.6 psum.14
  33.8 9.1 %reduce-scatter.17.cloned.1.call-done = f32[128,64]{0,1:T(8,128)} async-done(((f32[256,64]{0,1:T(8,128)}), f32[128,64]{0,1:T(8,128)}) %reduce-scatter.17.cloned.1.call-update) | async-done | bytes 32784 | tf_op jit(solution)/shard_map/reduce_scatter | solution.py:67
  42.8 10.7 %reduce-scatter.21.cloned.1.call-done = f32[128,64]{0,1:T(8,128)} async-done(((f32[256,64]{0,1:T(8,128)}), f32[128,64]{0,1:T(8,128)}) %reduce-scatter.21.cloned.1.call-update) | async-done | bytes 32784 | tf_op jit(solution)/shard_map/reduce_scatter | solution.py:63
  53.6 10.7 %reduce-scatter.23.cloned.1.call-done = f32[128,64]{0,1:T(8,128)} async-done(((f32[256,64]{0,1:T(8,128)}), f32[128,64]{0,1:T(8,128)}) %reduce-scatter.23.cloned.1.call-update) | async-done | bytes 32784 | tf_op jit(solution)/shard_map/reduce_scatter | solution.py:68
  64.3 10.7 %reduce-scatter.13.cloned.1.call-done = f32[128,64]{0,1:T(8,128)} async-done(((f32[256,64]{0,1:T(8,128)}), f32[128,64]{0,1:T(8,128)}) %reduce-scatter.13.cloned.1.call-update) | async-done | bytes 32784 | tf_op jit(solution)/shard_map/reduce_scatter | solution.py:66
  82.3 46.1 %collective-permute-done = f32[256,2048]{1,0:T(8,128)S(1)} collective-permute-done((f32[256,2048]{1,0:T(8,128)S(1)}, f32[256,2048]{1,0:T(8,128)S(1)}, u32[]{:S(2)}, u32[]{:S(2)}) %collective-permute-start) | collective-permute-done | bytes 2097184 | tf_op jit(solution)/shard_map/ppermute | solution.py:98
  130.6 45.3 %collective-permute-done.1 = f32[256,2048]{1,0:T(8,128)S(1)} collective-permute-done((f32[256,2048]{1,0:T(8,128)S(1)}, f32[256,2048]{1,0:T(8,128)S(1)}, u32[]{:S(2)}, u32[]{:S(2)}) %collective-permute-start.1) | collective-permute-done | bytes 2097184 | tf_op jit(solution)/shard_map/ppermute | solution.py:98
  178.1 44.4 %collective-permute-done.2 = f32[256,2048]{1,0:T(8,128)S(1)} collective-permute-done((f32[256,2048]{1,0:T(8,128)S(1)}, f32[256,2048]{1,0:T(8,128)S(1)}, u32[]{:S(2)}, u32[]{:S(2)}) %collective-permute-start.2) | collective-permute-done | bytes 2097184 | tf_op jit(solution)/shard_map/ppermute | solution.py:98
  222.9 2.7 collective-permute-start.3
  225.6 88.5 %collective-permute-done.3 = f32[256,2048]{1,0:T(8,128)S(1)} collective-permute-done((f32[256,2048]{1,0:T(8,128)S(1)}, f32[256,2048]{1,0:T(8,128)S(1)}, u32[]{:S(2)}, u32[]{:S(2)}) %collective-permute-start.3) | collective-permute-done | bytes 2097184 | tf_op jit(solution)/shard_map/ppermute | solution.py:98
  328.2 5.6 copy.46
  336.5 10.9 %reduce-scatter.29.cloned.1.call-done = f32[128,64]{0,1:T(8,128)} async-done(((f32[256,64]{0,1:T(8,128)}), f32[128,64]{0,1:T(8,128)}) %reduce-scatter.29.cloned.1.call-update) | async-done | bytes 32784 | tf_op jit(solution)/shard_map/reduce_scatter | solution.py:67
  347.4 11.3 %reduce-scatter.33.cloned.1.call-done = f32[128,64]{0,1:T(8,128)} async-done(((f32[256,64]{0,1:T(8,128)}), f32[128,64]{0,1:T(8,128)}) %reduce-scatter.33.cloned.1.call-update) | async-done | bytes 32784 | tf_op jit(solution)/shard_map/reduce_scatter | solution.py:63
  358.7 10.9 %reduce-scatter.35.cloned.1.call-done = f32[128,64]{0,1:T(8,128)} async-done(((f32[256,64]{0,1:T(8,128)}), f32[128,64]{0,1:T(8,128)}) %reduce-scatter.35.cloned.1.call-update) | async-done | bytes 32784 | tf_op jit(solution)/shard_map/reduce_scatter | solution.py:68
  369.6 10.7 %reduce-scatter.25.cloned.1.call-done = f32[128,64]{0,1:T(8,128)} async-done(((f32[256,64]{0,1:T(8,128)}), f32[128,64]{0,1:T(8,128)}) %reduce-scatter.25.cloned.1.call-update) | async-done | bytes 32784 | tf_op jit(solution)/shard_map/reduce_scatter | solution.py:66
  389.5 46.1 %collective-permute-done.4 = f32[256,2048]{1,0:T(8,128)S(1)} collective-permute-done((f32[256,2048]{1,0:T(8,128)S(1)}, f32[256,2048]{1,0:T(8,128)S(1)}, u32[]{:S(2)}, u32[]{:S(2)}) %collective-permute-start.4) | collective-permute-done | bytes 2097184 | tf_op jit(solution)/shard_map/ppermute | solution.py:98
  437.8 45.3 %collective-permute-done.5 = f32[256,2048]{1,0:T(8,128)S(1)} collective-permute-done((f32[256,2048]{1,0:T(8,128)S(1)}, f32[256,2048]{1,0:T(8,128)S(1)}, u32[]{:S(2)}, u32[]{:S(2)}) %collective-permute-start.5) | collective-permute-done | bytes 2097184 | tf_op jit(solution)/shard_map/ppermute | solution.py:98
  485.8 43.9 %collective-permute-done.6 = f32[256,2048]{1,0:T(8,128)S(1)} collective-permute-done((f32[256,2048]{1,0:T(8,128)S(1)}, f32[256,2048]{1,0:T(8,128)S(1)}, u32[]{:S(2)}, u32[]{:S(2)}) %collective-permute-start.6) | collective-permute-done | bytes 2097184 | tf_op jit(solution)/shard_map/ppermute | solution.py:98
  531.2 2.6 collective-permute-start.7
  539.3 10.1 %copy.24 = f32[2,128,1,4096]{3,2,1,0:T(1,128)} copy(f32[2,128,1,4096]{1,3,2,0:T(8,128)} %pad_maximum_fusion) | data formatting | bytes 8388608
  549.4 73.3 %collective-permute-done.7 = f32[256,2048]{1,0:T(8,128)} collective-permute-done((f32[256,2048]{1,0:T(8,128)}, f32[256,2048]{1,0:T(8,128)}, u32[]{:S(2)}, u32[]{:S(2)}) %collective-permute-start.7) | collective-permute-done | bytes 2097184 | tf_op jit(solution)/shard_map/ppermute | solution.py:98
  622.7 3.7 fusion.5
  (123 shorter events, 60.1 us)
Async XLA Ops:
  7.2 5.8 copy-start.2
  7.2 26.6 %reduce-scatter.19.cloned.1.call-start = ((), (), s32[]{:S(2)}) async-start(), calls=%async_computation.15 | async-start | bytes 98304 | tf_op jit(solution)/shard_map/reduce_scatter | solution.py:65
  10.5 23.3 %reduce-scatter.15.cloned.1.call-start = ((), (), s32[]{:S(2)}) async-start(), calls=%async_computation.13 | async-start | bytes 98304 | tf_op jit(solution)/shard_map/reduce_scatter | solution.py:64
  12.9 29.9 %reduce-scatter.17.cloned.1.call-start = ((), (), s32[]{:S(2)}) async-start(), calls=%async_computation.14 | async-start | bytes 98304 | tf_op jit(solution)/shard_map/reduce_scatter | solution.py:67
  14.1 39.5 %reduce-scatter.21.cloned.1.call-start = ((), (), s32[]{:S(2)}) async-start(), calls=%async_computation.16 | async-start | bytes 98304 | tf_op jit(solution)/shard_map/reduce_scatter | solution.py:63
  15.2 49.1 %reduce-scatter.23.cloned.1.call-start = ((), (), s32[]{:S(2)}) async-start(), calls=%async_computation.17 | async-start | bytes 98304 | tf_op jit(solution)/shard_map/reduce_scatter | solution.py:68
  16.4 58.7 %reduce-scatter.13.cloned.1.call-start = ((), (), s32[]{:S(2)}) async-start(), calls=%async_computation.12 | async-start | bytes 98304 | tf_op jit(solution)/shard_map/reduce_scatter | solution.py:66
  17.5 8.2 %copy-start.5 = (f32[2,64]{1,0:T(2,128)S(1)}, f32[2,64]{1,0:T(2,128)}, u32[]{:S(2)}) copy-start(f32[2,64]{1,0:T(2,128)} %param.20) | copy-start | bytes 1540
  17.6 8.1 %copy-start.6 = (f32[2,64]{1,0:T(2,128)S(1)}, f32[2,64]{1,0:T(2,128)}, u32[]{:S(2)}) copy-start(f32[2,64]{1,0:T(2,128)} %param.21) | copy-start | bytes 1540
  17.6 318.8 %reduce-scatter.31.cloned.1.call-start = ((), (), s32[]{:S(2)}) async-start(), calls=%async_computation.21 | async-start | bytes 98304 | tf_op jit(solution)/shard_map/reduce_scatter | solution.py:65
  80.6 47.9 %collective-permute-start = (f32[256,2048]{1,0:T(8,128)S(1)}, f32[256,2048]{1,0:T(8,128)S(1)}, u32[]{:S(2)}, u32[]{:S(2)}) collective-permute-start(f32[256,2048]{1,0:T(8,128)S(1)} %fusion.38), channel_id=1, source_target_pairs={{0,2},{2,0},{4,6},{6,4},{8,10},{10,8},{12,14},{14,12},{16,18},{18,... | collective-permute-start | bytes 6291464 | tf_op jit(solution)/shard_map/ppermute | solution.py:98
  128.8 47.1 %collective-permute-start.1 = (f32[256,2048]{1,0:T(8,128)S(1)}, f32[256,2048]{1,0:T(8,128)S(1)}, u32[]{:S(2)}, u32[]{:S(2)}) collective-permute-start(f32[256,2048]{1,0:T(8,128)S(1)} %add.197), channel_id=1, source_target_pairs={{0,4},{2,6},{4,0},{6,2},{8,12},{10,14},{12,8},{14,10},{16,20},{18,... | collective-permute-start | bytes 6291464 | tf_op jit(solution)/shard_map/ppermute | solution.py:98
  176.2 46.3 %collective-permute-start.2 = (f32[256,2048]{1,0:T(8,128)S(1)}, f32[256,2048]{1,0:T(8,128)S(1)}, u32[]{:S(2)}, u32[]{:S(2)}) collective-permute-start(f32[256,2048]{1,0:T(8,128)S(1)} %add.198), channel_id=1, source_target_pairs={{0,8},{2,10},{4,12},{6,14},{8,0},{10,2},{12,4},{14,6},{16,24},{18,... | collective-permute-start | bytes 6291464 | tf_op jit(solution)/shard_map/ppermute | solution.py:98
  222.9 92.8 %copy-start.7 = (bf16[2,2048,64]{1,2,0:T(8,128)(2,1)S(1)}, bf16[2,2048,64]{1,2,0:T(8,128)(2,1)}, u32[]{:S(2)}) copy-start(bf16[2,2048,64]{1,2,0:T(8,128)(2,1)} %param.16) | copy-start | bytes 1572868
  222.9 91.2 %collective-permute-start.3 = (f32[256,2048]{1,0:T(8,128)S(1)}, f32[256,2048]{1,0:T(8,128)S(1)}, u32[]{:S(2)}, u32[]{:S(2)}) collective-permute-start(f32[256,2048]{1,0:T(8,128)S(1)} %add.199), channel_id=1, source_target_pairs={{0,16},{2,18},{4,20},{6,22},{8,24},{10,26},{12,28},{14,30},{16,0},... | collective-permute-start | bytes 6291464 | tf_op jit(solution)/shard_map/ppermute | solution.py:98
  316.8 19.7 %reduce-scatter.27.cloned.1.call-start = ((), (), s32[]{:S(2)}) async-start(), calls=%async_computation.19 | async-start | bytes 98304 | tf_op jit(solution)/shard_map/reduce_scatter | solution.py:64
  319.3 28.1 %reduce-scatter.29.cloned.1.call-start = ((), (), s32[]{:S(2)}) async-start(), calls=%async_computation.20 | async-start | bytes 98304 | tf_op jit(solution)/shard_map/reduce_scatter | solution.py:67
  321.7 37.0 %reduce-scatter.33.cloned.1.call-start = ((), (), s32[]{:S(2)}) async-start(), calls=%async_computation.22 | async-start | bytes 98304 | tf_op jit(solution)/shard_map/reduce_scatter | solution.py:63
  323.8 45.8 %reduce-scatter.35.cloned.1.call-start = ((), (), s32[]{:S(2)}) async-start(), calls=%async_computation.23 | async-start | bytes 98304 | tf_op jit(solution)/shard_map/reduce_scatter | solution.py:68
  326.1 54.3 %reduce-scatter.25.cloned.1.call-start = ((), (), s32[]{:S(2)}) async-start(), calls=%async_computation.18 | async-start | bytes 98304 | tf_op jit(solution)/shard_map/reduce_scatter | solution.py:66
  387.7 47.9 %collective-permute-start.4 = (f32[256,2048]{1,0:T(8,128)S(1)}, f32[256,2048]{1,0:T(8,128)S(1)}, u32[]{:S(2)}, u32[]{:S(2)}) collective-permute-start(f32[256,2048]{1,0:T(8,128)S(1)} %fusion.30), channel_id=1, source_target_pairs={{0,2},{2,0},{4,6},{6,4},{8,10},{10,8},{12,14},{14,12},{16,18},{18,... | collective-permute-start | bytes 6291464 | tf_op jit(solution)/shard_map/ppermute | solution.py:98
  435.9 47.1 %collective-permute-start.5 = (f32[256,2048]{1,0:T(8,128)S(1)}, f32[256,2048]{1,0:T(8,128)S(1)}, u32[]{:S(2)}, u32[]{:S(2)}) collective-permute-start(f32[256,2048]{1,0:T(8,128)S(1)} %add.213), channel_id=1, source_target_pairs={{0,4},{2,6},{4,0},{6,2},{8,12},{10,14},{12,8},{14,10},{16,20},{18,... | collective-permute-start | bytes 6291464 | tf_op jit(solution)/shard_map/ppermute | solution.py:98
  483.4 46.3 %collective-permute-start.6 = (f32[256,2048]{1,0:T(8,128)S(1)}, f32[256,2048]{1,0:T(8,128)S(1)}, u32[]{:S(2)}, u32[]{:S(2)}) collective-permute-start(f32[256,2048]{1,0:T(8,128)S(1)} %add.214), channel_id=1, source_target_pairs={{0,8},{2,10},{4,12},{6,14},{8,0},{10,2},{12,4},{14,6},{16,24},{18,... | collective-permute-start | bytes 6291464 | tf_op jit(solution)/shard_map/ppermute | solution.py:98
  531.2 91.5 %collective-permute-start.7 = (f32[256,2048]{1,0:T(8,128)}, f32[256,2048]{1,0:T(8,128)}, u32[]{:S(2)}, u32[]{:S(2)}) collective-permute-start(f32[256,2048]{1,0:T(8,128)} %add.215), channel_id=1, source_target_pairs={{0,16},{2,18},{4,20},{6,22},{8,24},{10,26},{12,28},{14,30},{16,0},... | collective-permute-start | bytes 6291464 | tf_op jit(solution)/shard_map/ppermute | solution.py:98
  (8 other events, 25.0 us)
Sparse Core Ops, SparseCore 0:
  10.8 10.2 reduce-scatter.18
  23.2 8.6 reduce-scatter.14
  34.2 8.6 reduce-scatter.16
  44.9 8.6 reduce-scatter.20
  55.6 8.6 reduce-scatter.22
  66.4 8.6 reduce-scatter.12
  316.9 8.6 reduce-scatter.30
  327.8 8.7 reduce-scatter.26
  338.7 8.6 reduce-scatter.28
  350.0 8.6 reduce-scatter.32
  360.9 8.6 reduce-scatter.34
  371.6 8.6 reduce-scatter.24
